TPU v7x, 32 devices: a whole 2x2x4 slice. The times are simulated.
32 devices in a mesh: sp: 4 (over z), tp: 8 (over y, x, core).
Axes of the slice: x: 2, y: 2, z: 4, core: 2. Of those that a mesh axis runs over, the one named last changes fastest.
Arguments:
- latent: bfloat16 [2048, 4096], P(('sp', 'tp')), may hold values from -6 to 6
- context: bfloat16 [512, 4096], P('sp'), may hold values from -6 to 6
- condition: float32 [4096], P('sp'), may hold values from -6 to 6
- context_cond: float32 [4096], P('sp'), may hold values from -6 to 6
- mod_weight: bfloat16 [4096, 12288], P('sp', 'tp'), may hold values from -0.09375 to 0.09375
- norm_gain: float32 [4096], replicated, may hold values from 0.1 to 1.9
- query_weight: bfloat16 [4096, 4096], P(None, 'tp'), may hold values from -0.09375 to 0.09375
- key_weight: bfloat16 [4096, 2048], P(None, 'tp'), may hold values from -0.09375 to 0.09375
- value_weight: bfloat16 [4096, 2048], P(None, 'tp'), may hold values from -0.09375 to 0.09375
- out_weight: bfloat16 [4096, 4096], P(None, 'tp'), may hold values from -0.375 to 0.375
- query_gain: float32 [64], replicated, may hold values from 1.2 to 6
- key_gain: float32 [64], replicated, may hold values from 1.2 to 6
- context_lift: float32 [64], P('tp'), may hold values from 0.5 to 2
Outputs:
- updated: bfloat16 [2048, 4096], P(('sp', 'tp'))
All inputs are finite; a program needn't handle non-finite values.
Results may differ from a plain program's by a relative error of at most 0.0085.
The roundings to bfloat16 on the way count: a program that leaves them out, or rounds other values in their place, can miss the bound.
Values may be sent and summed in bfloat16 or wider, within the bound.
A program may use at most 64 MiB of HBM per device.

v0:
```python
import jax
import jax.numpy as jnp
from jax import lax
from jax.sharding import PartitionSpec as P

GRID_W = 64


EPS = 1e-06


def modulate(row_block, gain_vec, mod_row, model_width):
    row_values = row_block.astype(jnp.float32)
    normal = row_values * lax.rsqrt(jnp.mean(row_values * row_values, axis=-1, keepdims=True) + EPS)
    shift_part = mod_row[:model_width]
    scale_part = mod_row[model_width : 2 * model_width]
    return (normal * gain_vec * (1.0 + scale_part) + shift_part).astype(jnp.bfloat16)


def head_norm(values, gain_vec):
    return values * lax.rsqrt(jnp.mean(values * values, axis=-1, keepdims=True) + EPS) * gain_vec


def rope_tables(positions, head_size):
    freq_count = head_size // 4
    inverse = 10000.0 ** (-jnp.arange(freq_count, dtype=jnp.float32) / freq_count)
    grid_row = (positions // GRID_W).astype(jnp.float32)
    grid_col = (positions % GRID_W).astype(jnp.float32)
    angles = jnp.concatenate([grid_row[:, None] * inverse, grid_col[:, None] * inverse], axis=-1)
    return (jnp.cos(angles), jnp.sin(angles))


def rotate(values, cos_table, sin_table):
    paired = values.reshape(values.shape[:-1] + (values.shape[-1] // 2, 2))
    even_part = paired[..., 0]
    odd_part = paired[..., 1]
    cos_wide = cos_table[:, None, :]
    sin_wide = sin_table[:, None, :]
    turned = jnp.stack(
        [even_part * cos_wide - odd_part * sin_wide, even_part * sin_wide + odd_part * cos_wide],
        axis=-1,
    )
    return turned.reshape(values.shape)


def local(
    latent,
    context,
    condition,
    context_cond,
    mod_weight,
    norm_gain,
    query_weight,
    key_weight,
    value_weight,
    out_weight,
    query_gain,
    key_gain,
    context_lift,
):
    model_width = latent.shape[1]
    head_size = query_gain.shape[0]
    query_count = query_weight.shape[1] // head_size
    kv_count = key_weight.shape[1] // head_size
    group_size = query_count // kv_count
    score_scale = head_size ** (-0.5)
    cond_pair = jax.nn.silu(jnp.stack([condition, context_cond])).astype(jnp.bfloat16)
    partial_mod = jnp.dot(cond_pair, mod_weight, preferred_element_type=jnp.float32)
    summed_mod = lax.psum(partial_mod, "sp")
    modulation = lax.all_gather(summed_mod, "tp", axis=1, tiled=True)
    normed = modulate(latent, norm_gain, modulation[0], model_width)
    block_first = lax.axis_index("sp") * (latent.shape[0] * lax.axis_size("tp"))
    gathered = lax.all_gather(normed, "tp", axis=0, tiled=True)
    row_count = gathered.shape[0]
    query_raw = jnp.dot(gathered, query_weight, preferred_element_type=jnp.float32)
    key_raw = jnp.dot(gathered, key_weight, preferred_element_type=jnp.float32)
    value_raw = jnp.dot(gathered, value_weight, preferred_element_type=jnp.float32)
    positions = block_first + jnp.arange(row_count, dtype=jnp.int32)
    cos_table, sin_table = rope_tables(positions, head_size)
    query_rot = rotate(
        head_norm(query_raw.reshape(row_count, query_count, head_size), query_gain),
        cos_table,
        sin_table,
    )
    key_rot = rotate(
        head_norm(key_raw.reshape(row_count, kv_count, head_size), key_gain), cos_table, sin_table
    )
    joined = jnp.concatenate(
        [
            query_rot.reshape(row_count, -1).astype(jnp.bfloat16),
            key_rot.reshape(row_count, -1).astype(jnp.bfloat16),
            value_raw.astype(jnp.bfloat16),
        ],
        axis=1,
    )
    query_cols = query_count * head_size
    kv_cols = kv_count * head_size
    queries = joined[:, :query_cols]
    keys_here = joined[:, query_cols : query_cols + kv_cols]
    values_here = joined[:, query_cols + kv_cols :]
    normed_ctx = modulate(context, norm_gain, modulation[1], model_width)
    key_raw = jnp.dot(normed_ctx, key_weight, preferred_element_type=jnp.float32)
    ctx_key = head_norm(key_raw.reshape(context.shape[0], kv_count, head_size), key_gain)
    ctx_value = jnp.dot(normed_ctx, value_weight, preferred_element_type=jnp.float32)
    own_keys = ctx_key.reshape(context.shape[0], -1).astype(jnp.bfloat16)
    own_values = ctx_value.astype(jnp.bfloat16)
    ctx_keys, ctx_values = (
        lax.all_gather(own_keys, "sp", axis=0, tiled=True),
        lax.all_gather(own_values, "sp", axis=0, tiled=True),
    )
    query_rows = queries.shape[0]
    grouped = queries.reshape(query_rows, kv_count, group_size, head_size)
    lift_rows = context_lift.reshape(kv_count, group_size)
    zero_lift = jnp.zeros_like(lift_rows)

    def absorb(carry_state, key_block, value_block, offset):
        running_max, denom, numer = carry_state
        key_heads = key_block.reshape(-1, kv_count, head_size)
        value_heads = value_block.reshape(-1, kv_count, head_size)
        scores = jnp.einsum(
            "qhgd,khd->hgqk", grouped, key_heads, preferred_element_type=jnp.float32
        )
        scores = scores * score_scale + offset[:, :, None, None]
        new_max = jnp.maximum(running_max, jnp.max(scores, axis=-1))
        expo = jnp.exp(scores - new_max[..., None])
        rescale = jnp.exp(running_max - new_max)
        denom = denom * rescale + jnp.sum(expo, axis=-1)
        numer = numer * rescale[..., None] + jnp.einsum(
            "hgqk,khd->hgqd",
            expo.astype(jnp.bfloat16),
            value_heads,
            preferred_element_type=jnp.float32,
        )
        return (new_max, denom, numer)

    def sweep(carry_state, key_rows, value_rows, offset):
        row_count = key_rows.shape[0]
        block_size = 512
        if block_size == row_count:
            return absorb(carry_state, key_rows, value_rows, offset)
        key_blocks = key_rows.reshape(row_count // block_size, block_size, -1)
        value_blocks = value_rows.reshape(row_count // block_size, block_size, -1)

        def absorb_block(state_now, key_value):
            return (absorb(state_now, key_value[0], key_value[1], offset), None)

        final_state, unused = lax.scan(absorb_block, carry_state, (key_blocks, value_blocks))
        return final_state

    initial = (
        jnp.full((kv_count, group_size, query_rows), -jnp.inf, jnp.float32),
        jnp.zeros((kv_count, group_size, query_rows), jnp.float32),
        jnp.zeros((kv_count, group_size, query_rows, head_size), jnp.float32),
    )
    after_context = sweep(initial, ctx_keys, ctx_values, lift_rows)
    gathered = (
        lax.all_gather(keys_here, "sp", axis=0, tiled=True),
        lax.all_gather(values_here, "sp", axis=0, tiled=True),
    )
    running_max, denom, numer = sweep(after_context, gathered[0], gathered[1], zero_lift)
    attended = (numer / denom[..., None]).astype(jnp.bfloat16)
    attended = attended.transpose(2, 0, 1, 3).reshape(query_rows, query_cols)
    mixed_cols = jnp.dot(
        lax.all_gather(attended, "tp", axis=1, tiled=True),
        out_weight,
        preferred_element_type=jnp.float32,
    )
    mixed_rows = lax.all_to_all(
        mixed_cols.astype(jnp.bfloat16), "tp", split_axis=0, concat_axis=1, tiled=True
    )
    gate_lat = modulation[0, 2 * model_width :]
    return (latent.astype(jnp.float32) + gate_lat * mixed_rows.astype(jnp.float32)).astype(
        jnp.bfloat16
    )


def solution(mesh):
    return jax.shard_map(
        local,
        mesh=mesh,
        in_specs=(
            P(("sp", "tp"), None),
            P("sp", None),
            P("sp"),
            P("sp"),
            P("sp", "tp"),
            P(),
            P(None, "tp"),
            P(None, "tp"),
            P(None, "tp"),
            P(None, "tp"),
            P(),
            P(),
            P("tp"),
        ),
        out_specs=P(("sp", "tp"), None),
        check_vma=False,
    )
```

profile of v0, /device:TPU:1, one launch (start us, length us, event | category | flops | bytes accessed | tf_op | source)
XLA Modules:
  0.0 257.5 jit_solution(14006119027118180818)
XLA Ops:
  9.8 16.0 %psum.7 = f32[2,1536]{1,0:T(2,128)S(1)} all-reduce(f32[2,1536]{1,0:T(2,128)S(1)} %fusion.36), channel_id=1, replica_groups=mesh['sp'=4,'tp'=8] {'sp'}, use_global_device_ids=true, to_apply=%region_0.1 | all-reduce | flops 3072 | bytes 24576 | tf_op jit(solution)/shard_map/psum | solution.py:69
  25.9 13.5 %all_gather.21 = f32[2,12288]{1,0:T(2,128)S(1)} all-gather(f32[2,1536]{1,0:T(2,128)S(1)} %psum.7), channel_id=1, replica_groups=mesh['sp'=4,'tp'=8] {'tp'}, dimensions={1}, use_global_device_ids=true | all-gather | bytes 110592 | tf_op jit(solution)/shard_map/all_gather | solution.py:70
  40.0 2.1 fusion.28
  45.4 2.7 %convolution_convert_fusion.2 = bf16[128,256]{1,0:T(8,128)(2,1)S(1)} fusion(bf16[4096,256]{1,0:T(8,128)(2,1)} %param.23, bf16[128,4096]{1,0:T(8,128)(2,1)} %param.16, f32[4096]{0:T(1024)S(1)} %bitcast.146, f32[4096]{0:T(1024)S(1)} %bitcast.148, f32[4096]{0:T(1024)S(1)} %copy-done.7, f32[128]{0:T(128)S(1)} %add_rsqrt_fusion.4), kind=kOutput, calls=%fused_computation.34 | convolution fusion | flops 271613952 | bytes 3260928 | tf_op jit(solution)/shard_map/dot_general | solution.py:104
  48.1 11.0 %all_gather.24 = bf16[512,256]{1,0:T(8,128)(2,1)S(1)} all-gather(bf16[128,256]{1,0:T(8,128)(2,1)S(1)} %convolution_convert_fusion.2), channel_id=1, replica_groups=mesh['sp'=4,'tp'=8] {'sp'}, dimensions={0}, use_global_device_ids=true | all-gather | bytes 327680 | tf_op jit(solution)/shard_map/all_gather | solution.py:109
  59.9 3.1 %fusion.49 = (f32[128,256]{1,0:T(8,128)S(1)}, f32[128,256]{1,0:T(8,128)S(1)}) fusion(bf16[4096,256]{1,0:T(8,128)(2,1)} %param.22, bf16[128,4096]{1,0:T(8,128)(2,1)} %param.16, f32[4096]{0:T(1024)} %bitcast.147, f32[4096]{0:T(1024)} %bitcast.149, f32[4096]{0:T(1024)} %param.20, f32[128]{0:T(128)S(1)} %add_rsqrt_fusion.4), kind=kOutput, calls=%fused_computation.92 | convolution fusion | flops 271613952 | bytes 3457536 | tf_op jit(solution)/shard_map/dot_general | solution.py:102
  63.3 11.8 %all_gather.22 = bf16[512,256]{1,0:T(8,128)(2,1)} all-gather(bf16[128,256]{1,0:T(8,128)(2,1)S(1)} %multiply_convert_fusion), channel_id=1, replica_groups=mesh['sp'=4,'tp'=8] {'sp'}, dimensions={0}, use_global_device_ids=true | all-gather | bytes 327680 | tf_op jit(solution)/shard_map/all_gather | solution.py:108
  76.6 5.0 %bitcast_reduce_fusion.3 = (f32[512,4]{0,1:T(4,128)S(1)}, f32[512,256]{0,1:T(8,128)}) fusion(bf16[512,4096]{1,0:T(8,128)(2,1)} %all-gather.5.cloned.1.call-done, bf16[4096,256]{1,0:T(8,128)(2,1)} %param.22), kind=kOutput, calls=%fused_computation.46 | convolution fusion | flops 1074001920 | bytes 6823936 | tf_op jit(solution)/shard_map/dot_general | solution.py:76
  81.6 2.2 reshape.207
  89.0 7.4 %bitcast_reduce_fusion.2 = (f32[512,8]{0,1:T(8,128)}, f32[512,512]{0,1:T(8,128)}) fusion(bf16[512,4096]{1,0:T(8,128)(2,1)} %all-gather.5.cloned.1.call-done, bf16[4096,512]{1,0:T(8,128)(2,1)} %param.21), kind=kOutput, calls=%fused_computation.41 | convolution fusion | flops 2148003840 | bytes 9453568 | tf_op jit(solution)/shard_map/dot_general | solution.py:75
  96.4 2.8 %reshape.205 = f32[512,8,32,2]{0,3,2,1:T(2,128)} reshape(f32[512,512]{0,1:T(8,128)} %get-tuple-element.104) | data formatting | bytes 2097152 | tf_op jit(solution)/shard_map/reshape | solution.py:81
  103.1 2.0 pad_maximum_fusion
  105.1 2.1 convert_element_type.80
  107.1 4.8 %convolution_convert_fusion.1 = bf16[512,256]{1,0:T(8,128)(2,1)} fusion(bf16[512,4096]{1,0:T(8,128)(2,1)} %all-gather.5.cloned.1.call-done, bf16[4096,256]{1,0:T(8,128)(2,1)} %param.23), kind=kOutput, calls=%fused_computation.33 | convolution fusion | flops 1073872896 | bytes 6553600 | tf_op jit(solution)/shard_map/dot_general | solution.py:77
  112.3 2.5 bitcast_reduce_fusion.1
  116.6 2.9 %fusion.21 = f32[4,2,512,64]{2,3,1,0:T(8,128)} fusion(bf16[512,4,64,1]{0,2,3,1:T(8,128)(2,1)S(1)} %bitcast.142, f32[4,512,512,2]{2,1,3,0:T(8,128)S(1)} %get-tuple-element.106, f32[4,2,512]{2,1,0:T(2,128)S(1)} %get-tuple-element.171, f32[4,2]{1,0:T(4,128)S(1)} %add.177, f32[4,2,512]{2,1,0:T(2,128)S(1)} %get-tuple-element.97), kind=kOutput, calls=%fused_computation.31 | convolution fusion | flops 277086208 | bytes 9732128 | tf_op jit(solution)/shard_map/hgqk,khd->hgqd/dot_general | solution.py:128
  119.5 2.3 copy.36
  121.8 26.1 %all-gather.9.cloned.1.call-done = bf16[2048,256]{1,0:T(8,128)(2,1)} async-done(((bf16[512,256]{1,0:T(8,128)(2,1)}), bf16[2048,256]{1,0:T(8,128)(2,1)}) %all-gather.9.cloned.1.call-update) | async-done | bytes 1048592 | tf_op jit(solution)/shard_map/all_gather | solution.py:158
  147.9 45.5 %while.14 = (s32[]{:T(128)}, f32[4,2,512]{2,1,0:T(2,128)S(1)}, f32[4,2,512]{2,1,0:T(2,128)S(1)}, f32[4,2,512,64]{2,3,1,0:T(8,128)}, bf16[4,512,256]{2,1,0:T(8,12...) while((s32[]{:T(128)}, f32[4,2,512]{2,1,0:T(2,128)S(1)}, ...), condition=%wide.region_11.12_spmd, body=%wide.region_8.11_spmd.sunk | while | flops 554180608 | bytes 40108212 | solution.py:147
  147.9 1.8 constant_dynamic-slice_fusion.3
  152.6 2.3 bitcast_reduce_fusion.6
  159.3 1.8 constant_dynamic-slice_fusion.3
  164.0 2.4 bitcast_reduce_fusion.6
  167.8 1.8 fusion.78
  170.6 1.8 constant_dynamic-slice_fusion.3
  175.4 2.3 bitcast_reduce_fusion.6
  182.0 1.8 constant_dynamic-slice_fusion.3
  186.7 2.3 bitcast_reduce_fusion.6
  193.4 2.1 divide_convert_fusion
  195.5 37.0 %all-gather.11.cloned.1.call-done = bf16[512,4096]{0,1:T(8,128)(2,1)} async-done(((bf16[512,512]{0,1:T(8,128)(2,1)}), bf16[512,4096]{0,1:T(8,128)(2,1)}) %all-gather.11.cloned.1.call-update) | async-done | bytes 4194320 | tf_op jit(solution)/shard_map/all_gather | solution.py:164
  232.5 5.8 %convolution_convert_fusion = bf16[512,512]{1,0:T(8,128)(2,1)S(1)} fusion(bf16[512,4096]{0,1:T(8,128)(2,1)} %all-gather.11.cloned.1.call-done, bf16[4096,512]{1,0:T(8,128)(2,1)} %param.24), kind=kOutput, calls=%fused_computation.32 | convolution fusion | flops 2147745792 | bytes 8912896 | tf_op jit(solution)/shard_map/dot_general | solution.py:163
  238.4 11.4 %all_to_all.13 = bf16[8,64,512]{2,1,0:T(8,128)(2,1)S(1)} all-to-all(bf16[8,64,512]{2,1,0:T(8,128)(2,1)S(1)} %bitcast.140), channel_id=1, replica_groups=mesh['sp'=4,'tp'=8] {'tp'}, dimensions={0} | all-to-all | bytes 1048576 | tf_op jit(solution)/shard_map/all_to_all | solution.py:168
  (117 shorter events, 48.4 us)
Async XLA Ops:
  6.5 2.1 copy-start
  6.5 38.8 %copy-start.7 = (f32[4096]{0:T(1024)S(1)}, f32[4096]{0:T(1024)}, u32[]{:S(2)}) copy-start(f32[4096]{0:T(1024)} %param.20) | copy-start | bytes 49156
  6.5 35.7 %copy-start.11 = (f32[8]{0:T(128)S(1)}, f32[8]{0:T(128)}, u32[]{:S(2)}) copy-start(f32[8]{0:T(128)} %param.27) | copy-start | bytes 100
  6.5 35.8 %copy-start.10 = (f32[64]{0:T(128)S(1)}, f32[64]{0:T(128)}, u32[]{:S(2)}) copy-start(f32[64]{0:T(128)} %param.26) | copy-start | bytes 772
  6.5 36.6 %copy-start.12 = (f32[64]{0:T(128)S(1)}, f32[64]{0:T(128)}, u32[]{:S(2)}) copy-start(f32[64]{0:T(128)} %param.25) | copy-start | bytes 772
  6.5 70.0 %all-gather.5.cloned.1.call-start = ((), (), s32[]{:S(2)}) async-start(), calls=%async_computation.1 | async-start | bytes 4718592 | tf_op jit(solution)/shard_map/all_gather | solution.py:73
  40.0 19.0 %copy-start.8 = (f32[1,4096]{1,0:T(1,128)}, f32[1,4096]{1,0:T(1,128)S(1)}, u32[]{:S(2)}) copy-start(f32[1,4096]{1,0:T(1,128)S(1)} %get-tuple-element.93) | copy-start | bytes 49156
  40.0 19.0 %copy-start.9 = (f32[1,4096]{1,0:T(1,128)}, f32[1,4096]{1,0:T(1,128)S(1)}, u32[]{:S(2)}) copy-start(f32[1,4096]{1,0:T(1,128)S(1)} %get-tuple-element.94) | copy-start | bytes 49156
  42.2 77.3 %all-gather.7.cloned.1.call-start = ((), (), s32[]{:S(2)}) async-start(), calls=%async_computation.2 | async-start | bytes 1310720 | tf_op jit(solution)/shard_map/all_gather | solution.py:157
  88.7 59.1 %all-gather.9.cloned.1.call-start = ((), (), s32[]{:S(2)}) async-start(), calls=%async_computation.3 | async-start | bytes 1310720 | tf_op jit(solution)/shard_map/all_gather | solution.py:158
  112.0 120.5 %all-gather.11.cloned.1.call-start = ((), (), s32[]{:S(2)}) async-start(), calls=%async_computation.4 | async-start | bytes 4718592 | tf_op jit(solution)/shard_map/all_gather | solution.py:164
  114.8 1.8 copy-start.5
  155.0 1.4 copy-start.1
  155.0 1.4 copy-start.3
  158.3 1.0 copy-start.2
  166.4 1.4 copy-start.1
  166.4 1.4 copy-start.3
  169.6 1.0 copy-start.2
  177.7 1.4 copy-start.1
  177.7 1.4 copy-start.3
  181.0 1.0 copy-start.2
  189.1 1.4 copy-start.1
  189.1 1.4 copy-start.3
  192.4 1.0 copy-start.2
  238.3 11.7 %copy-start.4 = (bf16[64,4096]{1,0:T(8,128)(2,1)S(1)}, bf16[64,4096]{1,0:T(8,128)(2,1)}, u32[]{:S(2)}) copy-start(bf16[64,4096]{1,0:T(8,128)(2,1)} %param.15) | copy-start | bytes 1572868
  238.4 11.7 %copy-start.6 = (f32[1,4096]{1,0:T(1,128)S(1)}, f32[1,4096]{1,0:T(1,128)}, u32[]{:S(2)}) copy-start(f32[1,4096]{1,0:T(1,128)} %get-tuple-element.90) | copy-start | bytes 49156
Sparse Core Ops, SparseCore 0:
  42.3 33.7 all-gather.4
  88.9 30.0 all-gather.6
  120.5 27.3 all-gather.8
  195.6 36.8 all-gather.10
where the time goes:
time: 260 us; the launch traced here: 257 us
  blocking collectives  63.8 us (25%)
  waiting for transfers between devices  63.2 us (24%)
  matrix products  52.1 us (20%)
  local copies, waits for them, and re-layouts  38.4 us (15%)
  other arithmetic  25.7 us (10%)
  between operations  13.4 us (5%)
    all_gather x1, waiting for transfers between devices, local(): lax.all_gather(attended, 'tp', axis=1, tiled=True)  37 us
    all_gather x1, waiting for transfers between devices, local(): lax.all_gather(values_here, 'sp', axis=0, tiled=True)  26.1 us
    dynamic_slice x12, local copies, waits for them, and re-layouts, sweep(): lax.scan(absorb_block, carry_state, (key_blocks, value_blocks))  18.9 us
    psum x1, blocking collectives, local(): summed_mod = lax.psum(partial_mod, 'sp')  16 us
    all_gather x1, blocking collectives, local(): modulation = lax.all_gather(summed_mod, 'tp', axis=1, tiled=True)  13.5 us
    dot_general x5, matrix products, absorb(): jnp.einsum('qhgd,khd->hgqk', grouped, key_heads, preferred_element_type=j...  11.9 us
    all_gather x1, blocking collectives, local(): lax.all_gather(own_keys, 'sp', axis=0, tiled=True)  11.8 us
    all_to_all x1, blocking collectives, local(): lax.all_to_all(mixed_cols.astype(jnp.bfloat16), 'tp', split_axis=0, conca...  11.4 us
  transfers between devices with their start and end apart: 4, of which 2 were waited for; matrix products, arithmetic and copies ran while one was open for 17% of the time, Pallas kernels for 0%

commit v1 on v0

v1 whole, which is shorter than its diff:
```python
import functools

import jax
import jax.numpy as jnp
from jax import lax
from jax.experimental import pallas as pl
from jax.experimental.pallas import tpu as pltpu
from jax.sharding import PartitionSpec as P

GRID_W = 64
EPS = 1e-06
MESH = pl.DeviceIdType.MESH
ANY = pl.BlockSpec(memory_space=pl.ANY)
VMEM = pl.BlockSpec(memory_space=pltpu.VMEM)
SMEM = pl.BlockSpec(memory_space=pltpu.SMEM)
BF16 = jnp.bfloat16
F32 = jnp.float32


def remote(src, dst, send, recv, index, axis, peer):
    return pltpu.make_async_remote_copy(
        src_ref=src, dst_ref=dst, send_sem=send.at[index], recv_sem=recv.at[index],
        device_id={axis: peer}, device_id_type=MESH,
    )


def greet(peers):
    barrier = pltpu.get_barrier_semaphore()
    for axis, peer in peers:
        pl.semaphore_signal(barrier, inc=1, device_id={axis: peer}, device_id_type=MESH)
    pl.semaphore_wait(barrier, len(peers))


def others(axis, count):
    me = lax.axis_index(axis)
    return [(axis, lax.rem(me + step, count)) for step in range(1, count)]


def gather_sems(count):
    return 13 if count == 8 else max(count - 1, 1)


class Gather:
    def __init__(self, count, own, full, send, recv):
        self.count, self.own, self.full, self.send, self.recv = count, own, full, send, recv
        self.me = lax.axis_index("tp")
        self.half = own.shape[0] // 2
        me = self.me
        if count == 8:
            self.core, self.x, self.y = me % 2, (me // 2) % 2, me // 4
            self.sib = me + 1 - 2 * self.core
            self.step = 1 - 2 * self.core
            self.xn = me + 2 - 4 * self.x
            self.yn = me + 4 - 8 * self.y
            self.dn = self.xn + 4 - 8 * self.y

    def part(self, ref, which):
        return ref if which is None else ref.at[pl.ds(which * self.half, self.half)]

    def copy(self, index):
        me, xn, yn, dn, sib = self.me, self.xn, self.yn, self.dn, self.sib
        origin, half, peer = {
            0: (me, 0, xn), 1: (me, 1, xn), 2: (me, 0, yn), 3: (me, 1, yn), 4: (me, None, sib),
            5: (xn, 1, yn), 6: (yn, 0, xn),
            7: (xn, 0, sib), 8: (xn, 1, sib), 9: (yn, 0, sib), 10: (yn, 1, sib),
            11: (dn, 0, sib), 12: (dn, 1, sib),
        }[index]
        source = self.own if index < 5 else self.full.at[origin]
        return remote(self.part(source, half), self.part(self.full.at[origin], half), self.send, self.recv, index, "tp", peer)

    def wait_recv(self, index):
        xn, yn, dn, sib, step = self.xn, self.yn, self.dn, self.sib, self.step
        origin, half = {
            0: (xn, 0), 1: (xn, 1), 2: (yn, 0), 3: (yn, 1), 4: (sib, None), 5: (dn, 1), 6: (dn, 0),
            7: (xn + step, 0), 8: (xn + step, 1), 9: (yn + step, 0), 10: (yn + step, 1),
            11: (dn + step, 0), 12: (dn + step, 1),
        }[index]
        ref = self.part(self.full.at[origin], half)
        remote(ref, ref, self.send, self.recv, index, "tp", sib).wait_recv()

    def direct(self, step):
        peer = lax.rem(self.me + step, self.count)
        return remote(self.own, self.full.at[self.me], self.send, self.recv, step - 1, "tp", peer)

    def start(self):
        if self.count == 8:
            for index in (1, 2, 0, 3, 4):
                self.copy(index).start()
        else:
            for step in range(1, self.count):
                self.direct(step).start()

    def before(self, index):
        if self.count != 8:
            @pl.when(index == 0)
            def _():
                for step in range(1, self.count):
                    origin = lax.rem(self.me - step + self.count, self.count)
                    ref = self.full.at[origin]
                    remote(ref, ref, self.send, self.recv, step - 1, "tp", origin).wait_recv()
            return

        @pl.when(index == 0)
        def _():
            self.wait_recv(4)

        @pl.when(index == 1)
        def _():
            for arrived, then in ((1, (5, 8)), (2, (6, 9)), (0, (7,)), (3, (10,))):
                self.wait_recv(arrived)
                for nxt in then:
                    self.copy(nxt).start()
            self.wait_recv(7)
            self.wait_recv(8)

        @pl.when(index == 2)
        def _():
            self.wait_recv(9)
            self.wait_recv(10)

        @pl.when(index == 3)
        def _():
            self.wait_recv(5)
            self.copy(12).start()
            self.wait_recv(6)
            self.copy(11).start()
            self.wait_recv(12)
            self.wait_recv(11)

    def chip(self, index):
        if self.count == 8:
            return ((self.y + index // 2) % 2) * 2 + (self.x + index) % 2
        return index

    def finish(self):
        if self.count == 8:
            for index in range(13):
                self.copy(index).wait_send()
        else:
            for step in range(1, self.count):
                self.direct(step).wait_send()


def front_kernel(sp, tp, head, stacked, lat, ctx, partial, gain, cos, sin, gains, *rest):
    weights, rest = rest[: 1 if stacked else 3], rest[1 if stacked else 3 :]
    qkv, gate, full, normed, wide, parts, total, mod, gsc, shf, send, recv, psend, precv, msend, mrecv, local = rest
    s, f = lax.axis_index("sp"), lax.axis_index("tp")
    rows, model = lat.shape
    width = wide.shape[2]
    slots = wide.shape[0]
    tile = 2 * rows
    mcols = partial.shape[1]
    copies = []
    if stacked:
        copies.append(pltpu.make_async_copy(weights[0], wide, local.at[0]))
    else:
        groups = slots - 2
        for n in range(groups):
            copies.append(pltpu.make_async_copy(weights[0].at[:, n * width : (n + 1) * width], wide.at[n], local.at[n]))
        copies.append(pltpu.make_async_copy(weights[1], wide.at[groups], local.at[groups]))
        copies.append(pltpu.make_async_copy(weights[2], wide.at[groups + 1], local.at[groups + 1]))
    own = pltpu.make_async_copy(lat, full.at[f], local.at[slots])
    ctx_in = [
        pltpu.make_async_copy(ctx.at[pl.ds(n * rows, rows)], full.at[tp + n], local.at[slots + 1 + n]) for n in range(2)
    ]
    greet(others("tp", tp) + others("sp", sp))
    sends = []
    for step in range(1, sp):
        sends.append(remote(partial, parts.at[s], psend, precv, step - 1, "sp", lax.rem(s + step, sp)))
    for item in sends:
        item.start()
    gather = Gather(tp, lat, full, send, recv)
    gather.start()
    for item in ctx_in + [own] + copies:
        item.start()
    parts[s] = partial[...]
    for step in range(1, sp):
        origin = lax.rem(s - step + sp, sp)
        remote(parts.at[origin], parts.at[origin], psend, precv, step - 1, "sp", origin).wait_recv()
    summed = parts[0]
    for n in range(1, sp):
        summed = summed + parts[n]
    total[...] = summed
    here = pl.ds(pl.multiple_of(f * mcols, mcols), mcols)
    mod[:, here] = summed
    outs = []
    for step in range(1, tp):
        outs.append(remote(total, mod.at[:, here], msend, mrecv, step - 1, "tp", lax.rem(f + step, tp)))
    for item in outs:
        item.start()
    for step in range(1, tp):
        origin = lax.rem(f - step + tp, tp)
        ref = mod.at[:, pl.ds(pl.multiple_of(origin * mcols, mcols), mcols)]
        remote(ref, ref, msend, mrecv, step - 1, "tp", origin).wait_recv()
    for r in range(2):
        gsc[r] = gain[...] * (1.0 + mod[r : r + 1, model : 2 * model])
        shf[r] = mod[r : r + 1, :model]
    gate[...] = mod[0:1, 2 * model :]
    for item in ctx_in + copies:
        item.wait()
    own.wait()

    lane = lax.broadcasted_iota(jnp.int32, (tile, width), 1)
    even = lane % 2 == 0
    same = (
        lax.broadcasted_iota(jnp.int32, (width, width), 0) // head
        == lax.broadcasted_iota(jnp.int32, (width, width), 1) // head
    )
    ones = jnp.where(same, 1.0, 0.0).astype(BF16)
    step_rows = 16

    def roll(v, by):
        if width % 128 == 0:
            return pltpu.roll(v, by % width, axis=1)
        return jnp.concatenate([v[:, width - by % width :], v[:, : width - by % width]], axis=1)

    def widen(v):
        if width > v.shape[1]:
            return jnp.concatenate([v] * (width // v.shape[1]), axis=1)
        return v[:, :width]

    def one_tile(number, unused):
        order = number - 1

        @pl.when(number > 0)
        def _():
            gather.before(order)

        is_ctx = jnp.where(number == 0, 1, 0)
        chip = gather.chip(jnp.maximum(order, 0))
        chip = jnp.where(number == 0, tp // 2, chip)
        first = pl.multiple_of(chip * tile, tile)

        def norm_rows(j, unused):
            slot = chip * 2 + (j * step_rows) // rows
            row = pl.multiple_of((j * step_rows) % rows, step_rows)
            v = full[slot, pl.ds(row, step_rows), :].astype(F32)
            inv = lax.rsqrt(jnp.mean(v * v, axis=-1, keepdims=True) + EPS)
            out = v * inv * gsc[is_ctx] + shf[is_ctx]
            normed[pl.ds(pl.multiple_of(j * step_rows, step_rows), step_rows), :] = out.astype(BF16)
            return unused

        lax.fori_loop(0, tile // step_rows, norm_rows, 0)

        def one_slot(n, unused):
            y = jnp.dot(normed[...], wide[n], preferred_element_type=F32)

            @pl.when(n == slots - 1)
            def _():
                qkv[n, pl.ds(first, tile), :] = y.astype(BF16)

            @pl.when(n < slots - 1)
            def _():
                sq = y * y
                hi = sq.astype(BF16)
                lo = (sq - hi.astype(F32)).astype(BF16)
                mean = jnp.dot(hi, ones, preferred_element_type=F32) + jnp.dot(lo, ones, preferred_element_type=F32)
                u = y * lax.rsqrt(mean * (1.0 / head) + EPS) * gains[n]
                other = jnp.where(even, roll(u, -1), roll(u, 1))
                turned = u * widen(cos[pl.ds(first, tile), :]) + other * widen(sin[pl.ds(first, tile), :])
                qkv[n, pl.ds(first, tile), :] = turned.astype(BF16)

            return unused

        lax.fori_loop(jnp.where(number == 0, slots - 2, 0), slots, one_slot, 0)
        return unused

    lax.fori_loop(0, tp // 2 + 1, one_tile, 0)
    for item in sends + outs:
        item.wait_send()
    gather.finish()


def attend_kernel(sp, heads, kv_heads, head, lat_rows, qkv, lift, out, kvs, top, acc, send, recv, local):
    s = lax.axis_index("sp")
    slots, rows, width = qkv.shape
    group = heads // kv_heads
    ring = sp == 4
    right, left, far = (s + 1) % sp, (s + sp - 1) % sp, (s + 2) % sp
    greet([("sp", right), ("sp", left)] if ring else others("sp", sp))
    own = qkv.at[pl.ds(slots - 2, 2)]

    def ring_copy(index):
        which, origin, peer = {
            0: (0, s, right), 1: (1, s, right), 2: (1, s, left), 3: (0, s, left), 4: (0, left, right), 5: (1, right, left),
        }[index]
        source = qkv.at[slots - 2 + which] if index < 4 else kvs.at[origin, which]
        return remote(source, kvs.at[origin, which], send, recv, index, "sp", peer)

    def ring_wait(index):
        which, origin = {0: (0, left), 1: (1, left), 2: (1, right), 3: (0, right), 4: (0, far), 5: (1, far)}[index]
        ref = kvs.at[origin, which]
        remote(ref, ref, send, recv, index, "sp", right).wait_recv()

    def direct(step):
        return remote(own, kvs.at[s], send, recv, step - 1, "sp", lax.rem(s + step, sp))

    if ring:
        for index in (0, 2, 1, 3):
            ring_copy(index).start()
    else:
        for step in range(1, sp):
            direct(step).start()
    mine = pltpu.make_async_copy(own, kvs.at[s], local)
    mine.start()
    top[...] = jnp.full(top.shape, -1e30, F32)
    acc[...] = jnp.zeros(acc.shape, F32)
    mine.wait()
    q_tile = min(256, lat_rows)
    scale = head ** -0.5

    def block(b, unused):
        if ring:
            @pl.when(b == 1)
            def _():
                ring_wait(0)
                ring_copy(4).start()
                ring_wait(2)
                ring_copy(5).start()
                ring_wait(1)

            @pl.when(b == 2)
            def _():
                ring_wait(3)

            @pl.when(b == 3)
            def _():
                ring_wait(4)
                ring_wait(5)

            origin = (s + jnp.where(b == 1, sp - 1, jnp.where(b == 2, 1, jnp.where(b == 3, 2, 0)))) % sp
        else:
            @pl.when(b == 1)
            def _():
                for step in range(1, sp):
                    source = lax.rem(s - step + sp, sp)
                    remote(kvs.at[source], kvs.at[source], send, recv, step - 1, "sp", source).wait_recv()

            origin = (s + b) % sp

        def q_rows(t, unused):
            first = pl.multiple_of(t * q_tile, q_tile)
            at = pl.ds(first, q_tile)
            for h in range(kv_heads):
                k = kvs[origin, 0, :, h * head : (h + 1) * head]
                v = kvs[origin, 1, :, h * head : (h + 1) * head]
                v_wide = jnp.concatenate([v, jnp.ones((rows, head), BF16)], axis=1)
                for g in range(group):
                    n = h * group + g
                    slot, lane = (n * head) // width, (n * head) % width
                    q = qkv[slot, at, lane : lane + head]
                    scores = lax.dot_general(q, k, (((1,), (1,)), ((), ())), preferred_element_type=F32)
                    scores = scores * scale
                    offset = jnp.where(lax.broadcasted_iota(jnp.int32, (1, rows), 1) >= lat_rows, lift[n], 0.0)
                    scores = scores + offset
                    before = top[n, at, :]
                    now = jnp.maximum(before, jnp.max(scores, axis=-1, keepdims=True))
                    expo = jnp.exp(scores - now)
                    keep = jnp.exp(before - now)
                    top[n, at, :] = now
                    acc[n, at, :] = acc[n, at, :] * keep + jnp.dot(expo.astype(BF16), v_wide, preferred_element_type=F32)
            return unused

        lax.fori_loop(0, lat_rows // q_tile, q_rows, 0)
        return unused

    lax.fori_loop(0, sp, block, 0)

    def close(t, unused):
        at = pl.ds(pl.multiple_of(t * q_tile, q_tile), q_tile)
        for pair in range(heads // 2):
            two = [acc[2 * pair + n, at, :] for n in range(2)]
            two = [v[:, :head] / v[:, head:] for v in two]
            out[at, pair * 2 * head : (pair + 1) * 2 * head] = jnp.concatenate(two, axis=1).astype(BF16)
        return unused

    lax.fori_loop(0, lat_rows // q_tile, close, 0)
    if ring:
        for index in range(6):
            ring_copy(index).wait_send()
    else:
        for step in range(1, sp):
            direct(step).wait_send()


def back_kernel(tp, att, weight, lat, gate, out, full, wide, total, mixed, landed, send, recv, asend, arecv, local):
    f = lax.axis_index("tp")
    rows, cols = att.shape
    own_rows = lat.shape[0]
    out_cols = weight.shape[1]
    load = pltpu.make_async_copy(weight, wide, local.at[0])
    load.start()
    mine = pltpu.make_async_copy(att, full.at[f], local.at[1])
    mine.start()
    greet(others("tp", tp))
    gather = Gather(tp, att, full, send, recv)
    gather.start()
    total[...] = jnp.zeros(total.shape, F32)
    mine.wait()
    load.wait()
    r_tile = min(256, rows)

    def chip_step(index, unused):
        gather.before(index)
        chip = gather.chip(index)

        def row_step(t, unused):
            at = pl.ds(pl.multiple_of(t * r_tile, r_tile), r_tile)
            value = total[at, :]
            for n in range(2):
                source = chip * 2 + n
                depth = pl.ds(pl.multiple_of(source * cols, cols), cols)
                value = value + jnp.dot(full[source, at, :], wide[depth, :], preferred_element_type=F32)
            total[at, :] = value
            return unused

        lax.fori_loop(0, rows // r_tile, row_step, 0)
        return unused

    lax.fori_loop(0, tp // 2, chip_step, 0)
    for peer in range(tp):
        mixed[peer] = total[peer * own_rows : (peer + 1) * own_rows, :].astype(BF16)
    sends = []
    for step in range(1, tp):
        peer = lax.rem(f + step, tp)
        sends.append(remote(mixed.at[peer], landed.at[f], asend, arecv, step - 1, "tp", peer))
    for item in sends:
        item.start()
    landed[f] = mixed[f]
    for step in range(1, tp):
        origin = lax.rem(f - step + tp, tp)
        remote(landed.at[origin], landed.at[origin], asend, arecv, step - 1, "tp", origin).wait_recv()
    for n in range(tp):
        at = slice(n * out_cols, (n + 1) * out_cols)
        out[:, at] = (lat[:, at].astype(F32) + gate[:, at] * landed[n].astype(F32)).astype(BF16)
    for item in sends:
        item.wait_send()
    gather.finish()


def tables(first, count, extra, head):
    freqs = head // 4
    lane = jnp.arange(2 * head, dtype=jnp.int32) % head
    pair = lane // 2
    inverse = 10000.0 ** (-(pair % freqs).astype(F32) / freqs)
    sign = jnp.where(lane % 2 == 0, -1.0, 1.0)
    by_row = pair < freqs
    grid_rows = -(-count // GRID_W) + 1
    small = jnp.concatenate([jnp.arange(grid_rows, dtype=jnp.int32) + first // GRID_W, jnp.arange(GRID_W, dtype=jnp.int32)])
    angles = small.astype(F32)[:, None] * inverse
    cos, sin = lax.optimization_barrier((jnp.cos(angles), jnp.sin(angles) * sign))

    def spread(table, fill):
        if count % GRID_W == 0:
            row = jnp.broadcast_to(table[: count // GRID_W, None, :], (count // GRID_W, GRID_W, 2 * head))
            col = jnp.broadcast_to(table[None, grid_rows:, :], row.shape)
            both = jnp.where(by_row, row, col).reshape(count, 2 * head)
        else:
            spots = first + jnp.arange(count, dtype=jnp.int32)
            both = jnp.where(by_row, table[spots // GRID_W - first // GRID_W], table[grid_rows + spots % GRID_W])
        return jnp.concatenate([both, jnp.full((extra, 2 * head), fill, F32)])

    return spread(cos, 1.0), spread(sin, 0.0)


def local(sp, tp, latent, context, condition, context_cond, mod_weight, norm_gain, query_weight, key_weight,
          value_weight, out_weight, query_gain, key_gain, context_lift):
    rows, model = latent.shape
    ctx_rows = context.shape[0]
    head = query_gain.shape[0]
    heads = query_weight.shape[1] // head
    kv_heads = key_weight.shape[1] // head
    width = key_weight.shape[1]
    slots = query_weight.shape[1] // width + 2
    block = rows * tp
    keys = block + ctx_rows
    limit = 60 * 1024 * 1024
    cond_pair = jax.nn.silu(jnp.stack([condition, context_cond])).astype(BF16)
    partial = jnp.dot(cond_pair, mod_weight, preferred_element_type=F32)
    mcols = partial.shape[1]
    cos, sin = tables(lax.axis_index("sp") * block, block, ctx_rows, head)
    gains = jnp.stack([jnp.tile(query_gain, width // head)] * (slots - 2) + [jnp.tile(key_gain, width // head)] * 2)
    gains = gains.reshape(slots, 1, width)
    stacked = width % 128 != 0
    weights = [query_weight, key_weight, value_weight]
    if stacked:
        weights = [jnp.stack([query_weight[:, n * width : (n + 1) * width] for n in range(slots - 2)] + weights[1:])]
    dma = pltpu.SemaphoreType.DMA
    count = gather_sems(tp)
    qkv, gate = pl.pallas_call(
        functools.partial(front_kernel, sp, tp, head, stacked),
        name="front",
        out_shape=(jax.ShapeDtypeStruct((slots, keys, width), BF16), jax.ShapeDtypeStruct((1, model), F32)),
        in_specs=[ANY, ANY, VMEM, VMEM, VMEM, VMEM, VMEM] + [ANY] * len(weights),
        out_specs=(VMEM, VMEM),
        scratch_shapes=[
            pltpu.VMEM((tp + 2, rows, model), BF16),
            pltpu.VMEM((2 * rows, model), BF16),
            pltpu.VMEM((slots, model, width), BF16),
            pltpu.VMEM((sp, 2, mcols), F32),
            pltpu.VMEM((2, mcols), F32),
            pltpu.VMEM((2, mcols * tp), F32),
            pltpu.VMEM((2, 1, model), F32),
            pltpu.VMEM((2, 1, model), F32),
            dma((count,)), dma((count,)), dma((sp - 1,)), dma((sp - 1,)), dma((tp - 1,)), dma((tp - 1,)),
            dma((slots + 3,)),
        ],
        compiler_params=pltpu.CompilerParams(collective_id=0, has_side_effects=True, vmem_limit_bytes=limit),
    )(latent, context, partial, norm_gain.reshape(1, model), cos, sin, gains, *weights)
    attended = pl.pallas_call(
        functools.partial(attend_kernel, sp, heads, kv_heads, head, block),
        name="attend",
        out_shape=jax.ShapeDtypeStruct((block, heads * head), BF16),
        in_specs=[VMEM, SMEM],
        out_specs=VMEM,
        scratch_shapes=[
            pltpu.VMEM((sp, 2, keys, width), BF16),
            pltpu.VMEM((heads, block, 1), F32),
            pltpu.VMEM((heads, block, 2 * head), F32),
            dma((max(sp - 1, 6),)), dma((max(sp - 1, 6),)), dma,
        ],
        compiler_params=pltpu.CompilerParams(collective_id=1, has_side_effects=True, vmem_limit_bytes=limit),
    )(qkv, context_lift)
    return pl.pallas_call(
        functools.partial(back_kernel, tp),
        name="back",
        out_shape=jax.ShapeDtypeStruct((rows, model), BF16),
        in_specs=[VMEM, ANY, VMEM, VMEM],
        out_specs=VMEM,
        scratch_shapes=[
            pltpu.VMEM((tp, block, heads * head), BF16),
            pltpu.VMEM(out_weight.shape, BF16),
            pltpu.VMEM((block, out_weight.shape[1]), F32),
            pltpu.VMEM((tp, rows, out_weight.shape[1]), BF16),
            pltpu.VMEM((tp, rows, out_weight.shape[1]), BF16),
            dma((count,)), dma((count,)), dma((tp - 1,)), dma((tp - 1,)), dma((2,)),
        ],
        compiler_params=pltpu.CompilerParams(collective_id=2, has_side_effects=True, vmem_limit_bytes=limit),
    )(attended, out_weight, latent, gate)


def solution(mesh):
    return jax.shard_map(
        functools.partial(local, mesh.shape["sp"], mesh.shape["tp"]),
        mesh=mesh,
        in_specs=(
            P(("sp", "tp"), None),
            P("sp", None),
            P("sp"),
            P("sp"),
            P("sp", "tp"),
            P(),
            P(None, "tp"),
            P(None, "tp"),
            P(None, "tp"),
            P(None, "tp"),
            P(),
            P(),
            P("tp"),
        ),
        out_specs=P(("sp", "tp"), None),
        check_vma=False,
    )
```

time: 260 us -> 143 us (0.55)
  Pallas kernels: 0 us -> 134 us
  blocking collectives: 63.8 us -> 0 us
  waiting for transfers between devices: 63.2 us -> 0 us
  matrix products: 52.1 us -> 1.82 us
  local copies, waits for them, and re-layouts: 38.4 us -> 5.63 us
  other arithmetic: 25.7 us -> 0.38 us
  between operations: 13.4 us -> 0.09 us
    pallas_call x0 -> x3, Pallas kernels: none -> 134 us  [the longest x1 55.7 us: local(): pl.pallas_call(functools.partial(attend_kernel, sp, heads, kv_heads, head...]
    all_gather x4 -> x0, waiting for transfers between devices: 63.1 us -> none  [the longest x1 37 us: local(): lax.all_gather(attended, 'tp', axis=1, tiled=True)]
    dot_general x17 -> x1, matrix products: 52.1 us -> 1.82 us  [local(): partial = jnp.dot(cond_pair, mod_weight, preferred_element_type=F32)]
    all_gather x3 -> x0, blocking collectives: 36.3 us -> none  [the longest x1 13.5 us: local(): modulation = lax.all_gather(summed_mod, 'tp', axis=1, tiled=True)]
    dynamic_slice x12 -> x0, local copies, waits for them, and re-layouts: 18.9 us -> none  [sweep(): lax.scan(absorb_block, carry_state, (key_blocks, value_blocks))]
    psum x1 -> x0, blocking collectives: 16 us -> none  [local(): summed_mod = lax.psum(partial_mod, 'sp')]
    all_to_all x1 -> x0, blocking collectives: 11.4 us -> none  [local(): lax.all_to_all(mixed_cols.astype(jnp.bfloat16), 'tp', split_axis=0, conca...]
    reduce_sum x8 -> x0, other arithmetic: 10.3 us -> none  [the longest x5 7.33 us: absorb(): denom = denom * rescale + jnp.sum(expo, axis=-1)]
  transfers between devices with their start and end apart: 4 -> 0, of which waited for: 2 -> 0; matrix products, arithmetic and copies ran while one was open for 17% -> 0% of each run, Pallas kernels for 0% -> 0%
where the time goes in v1:
time: 143 us; the launch traced here: 142 us
  Pallas kernels  134 us (94%)
  local copies, waits for them, and re-layouts  5.63 us (4%)
  matrix products  1.82 us (1%)
    pallas_call x1, Pallas kernels, local(): pl.pallas_call(functools.partial(attend_kernel, sp, heads, kv_heads, head...  55.7 us
    pallas_call x1, Pallas kernels, local(): pl.pallas_call(functools.partial(front_kernel, sp, tp, head, stacked), na...  45.1 us
    pallas_call x1, Pallas kernels, local(): pl.pallas_call(functools.partial(back_kernel, tp), name='back', out_shape...  33.6 us

profile of v1, /device:TPU:1, one launch (start us, length us, event | category | flops | bytes accessed | tf_op | source)
XLA Modules:
  0.0 142.3 jit_solution(14129356594676832979)
XLA Ops:
  0.0 0.0 copy-start
  0.0 0.1 add_convert_fusion
  0.1 0.8 tile.4
  0.9 0.1 stack_tile.8
  1.0 0.7 tile.5
  1.7 0.1 stack_tile.9
  1.8 0.6 reshape.84.gains
  2.4 0.0 copy-done
  2.4 1.8 %fusion.2.partial = f32[2,1536]{1,0:T(2,128)} fusion(bf16[1024,1536]{1,0:T(8,128)(2,1)S(1)} %copy-done, f32[1,1024]{1,0:T(1,128)} %bitcast.13, f32[1,1024]{1,0:T(1,128)} %bitcast.14), kind=kOutput, calls=%fused_computation.8 | convolution fusion | flops 6303744 | bytes 3166208 | tf_op jit(solution)/shard_map/dot_general | solution.py:479
  4.2 0.2 fusion
  4.5 0.8 concatenate.15.sin
  5.3 0.7 concatenate.14.cos
  6.0 45.1 %front.1 = (bf16[4,640,256]{2,1,0:T(8,128)(2,1)}, f32[1,4096]{1,0:T(1,128)}) custom-call(bf16[64,4096]{1,0:T(8,128)(2,1)} %lat.3, bf16[128,4096]{1,0:T(8,128)(2,1)} %ctx.1, f32[2,1536]{1,0:T(2,128)} %fusion.2.partial, f32[1,4096]{1,0:T(1,128)} %bitcast.12, f32[640,128]{1,0:T(8,128)} %concatenate.14.cos, f32[640,128]{1,0:T(8,128)} %concatenate.15.sin, ...), custom_call_target="tpu_custom_call" | custom-call | tf_op jit(solution)/shard_map/front/pallas_call | solution.py:490
  51.1 55.7 %attend.1.att = bf16[512,512]{1,0:T(8,128)(2,1)} custom-call(bf16[4,640,256]{2,1,0:T(8,128)(2,1)} %get-tuple-element.11.qkv, f32[8]{0:T(128)} %lift.1), custom_call_target="tpu_custom_call" | custom-call | tf_op jit(solution)/shard_map/attend/pallas_call | solution.py:510
  106.9 33.6 %back.1 = bf16[64,4096]{1,0:T(8,128)(2,1)} custom-call(bf16[512,512]{1,0:T(8,128)(2,1)} %attend.1.att, bf16[4096,512]{1,0:T(8,128)(2,1)} %weight.1, bf16[64,4096]{1,0:T(8,128)(2,1)} %lat.3, f32[1,4096]{1,0:T(1,128)} %get-tuple-element.12.gate), custom_call_target="tpu_custom_call" | custom-call | tf_op jit(solution)/shard_map/back/pallas_call | solution.py:524
  140.5 1.9 %copy.15 = bf16[64,4096]{1,0:T(8,128)(2,1)} copy(bf16[64,4096]{1,0:T(8,128)(2,1)} %back.1) | data formatting | bytes 1048576
  (10 shorter events, 0.1 us)
Async XLA Ops:
  0.0 2.4 %copy-start = (bf16[1024,1536]{1,0:T(8,128)(2,1)S(1)}, bf16[1024,1536]{1,0:T(8,128)(2,1)}, u32[]{:S(2)}) copy-start(bf16[1024,1536]{1,0:T(8,128)(2,1)} %param.17) | copy-start | bytes 9437188

commit v2 on v1

v2 whole, which is shorter than its diff:
```python
import functools

import jax
import jax.numpy as jnp
from jax import lax
from jax.experimental import pallas as pl
from jax.experimental.pallas import tpu as pltpu
from jax.sharding import PartitionSpec as P

GRID_W = 64
EPS = 1e-06
MESH = pl.DeviceIdType.MESH
ANY = pl.BlockSpec(memory_space=pl.ANY)
VMEM = pl.BlockSpec(memory_space=pltpu.VMEM)
SMEM = pl.BlockSpec(memory_space=pltpu.SMEM)
BF16 = jnp.bfloat16
F32 = jnp.float32


def remote(src, dst, send, recv, index, axis, peer):
    return pltpu.make_async_remote_copy(
        src_ref=src, dst_ref=dst, send_sem=send.at[index], recv_sem=recv.at[index],
        device_id={axis: peer}, device_id_type=MESH,
    )


def greet(peers):
    barrier = pltpu.get_barrier_semaphore()
    for axis, peer in peers:
        pl.semaphore_signal(barrier, inc=1, device_id={axis: peer}, device_id_type=MESH)
    pl.semaphore_wait(barrier, len(peers))


def others(axis, count):
    me = lax.axis_index(axis)
    return [(axis, lax.rem(me + step, count)) for step in range(1, count)]


def gather_sems(count):
    return 13 if count == 8 else max(count - 1, 1)


class Gather:
    def __init__(self, count, own, full, send, recv):
        self.count, self.own, self.full, self.send, self.recv = count, own, full, send, recv
        self.me = lax.axis_index("tp")
        self.half = own.shape[0] // 2
        me = self.me
        if count == 8:
            self.core, self.x, self.y = me % 2, (me // 2) % 2, me // 4
            self.sib = me + 1 - 2 * self.core
            self.step = 1 - 2 * self.core
            self.xn = me + 2 - 4 * self.x
            self.yn = me + 4 - 8 * self.y
            self.dn = self.xn + 4 - 8 * self.y

    def part(self, ref, which):
        return ref if which is None else ref.at[pl.ds(which * self.half, self.half)]

    def copy(self, index):
        me, xn, yn, dn, sib = self.me, self.xn, self.yn, self.dn, self.sib
        origin, half, peer = {
            0: (me, 0, xn), 1: (me, 1, xn), 2: (me, 0, yn), 3: (me, 1, yn), 4: (me, None, sib),
            5: (xn, 1, yn), 6: (yn, 0, xn),
            7: (xn, 0, sib), 8: (xn, 1, sib), 9: (yn, 0, sib), 10: (yn, 1, sib),
            11: (dn, 0, sib), 12: (dn, 1, sib),
        }[index]
        source = self.own if index < 5 else self.full.at[origin]
        return remote(self.part(source, half), self.part(self.full.at[origin], half), self.send, self.recv, index, "tp", peer)

    def wait_recv(self, index):
        xn, yn, dn, sib, step = self.xn, self.yn, self.dn, self.sib, self.step
        origin, half = {
            0: (xn, 0), 1: (xn, 1), 2: (yn, 0), 3: (yn, 1), 4: (sib, None), 5: (dn, 1), 6: (dn, 0),
            7: (xn + step, 0), 8: (xn + step, 1), 9: (yn + step, 0), 10: (yn + step, 1),
            11: (dn + step, 0), 12: (dn + step, 1),
        }[index]
        ref = self.part(self.full.at[origin], half)
        remote(ref, ref, self.send, self.recv, index, "tp", sib).wait_recv()

    def direct(self, step):
        peer = lax.rem(self.me + step, self.count)
        return remote(self.own, self.full.at[self.me], self.send, self.recv, step - 1, "tp", peer)

    def start(self):
        if self.count == 8:
            for index in (1, 2, 4):
                self.copy(index).start()
        else:
            for step in range(1, self.count):
                self.direct(step).start()

    def second(self):
        if self.count == 8:
            for index in (0, 3):
                self.copy(index).start()

    def relay(self):
        if self.count == 8:
            for arrived, then in ((1, (5, 8)), (2, (6, 9))):
                self.wait_recv(arrived)
                for nxt in then:
                    self.copy(nxt).start()

    def before(self, index):
        if self.count != 8:
            @pl.when(index == 0)
            def _():
                for step in range(1, self.count):
                    origin = lax.rem(self.me - step + self.count, self.count)
                    ref = self.full.at[origin]
                    remote(ref, ref, self.send, self.recv, step - 1, "tp", origin).wait_recv()
            return

        @pl.when(index == 0)
        def _():
            self.wait_recv(4)

        @pl.when(index == 1)
        def _():
            for arrived, nxt in ((0, 7), (3, 10)):
                self.wait_recv(arrived)
                self.copy(nxt).start()
            self.wait_recv(7)
            self.wait_recv(8)

        @pl.when(index == 2)
        def _():
            self.wait_recv(9)
            self.wait_recv(10)

        @pl.when(index == 3)
        def _():
            self.wait_recv(5)
            self.copy(12).start()
            self.wait_recv(6)
            self.copy(11).start()
            self.wait_recv(12)
            self.wait_recv(11)

    def chip(self, index):
        if self.count == 8:
            return ((self.y + index // 2) % 2) * 2 + (self.x + index) % 2
        return index

    def finish(self):
        if self.count == 8:
            for index in range(13):
                self.copy(index).wait_send()
        else:
            for step in range(1, self.count):
                self.direct(step).wait_send()


def front_kernel(sp, tp, heads, kv_heads, head, stacked, lat, ctx, cond, mod_weight, gain, cos, sin, q_gain, k_gain, lift, *rest):
    weights, rest = rest[: 1 if stacked else 3], rest[1 if stacked else 3 :]
    (attended, gate, full, normed, wide, mod_wide, parts, partial, total, mod, gsc, shf, gains, q_all, kvs, top, acc,
     send, recv, psend, precv, msend, mrecv, zsend, zrecv, local) = rest
    s, f = lax.axis_index("sp"), lax.axis_index("tp")
    rows, model = lat.shape
    width = wide.shape[2]
    slots = wide.shape[0]
    groups = slots - 2
    tile = 2 * rows
    lat_rows = rows * tp
    keys = kvs.shape[2]
    mcols = partial.shape[1]
    tiles = tp // 2 + 1
    mod_in = pltpu.make_async_copy(mod_weight, mod_wide, local.at[slots + 3])
    mod_in.start()
    copies = []
    if stacked:
        copies.append(pltpu.make_async_copy(weights[0], wide, local.at[0]))
    else:
        for n in range(groups):
            copies.append(pltpu.make_async_copy(weights[0].at[:, n * width : (n + 1) * width], wide.at[n], local.at[n]))
        copies.append(pltpu.make_async_copy(weights[1], wide.at[groups], local.at[groups]))
        copies.append(pltpu.make_async_copy(weights[2], wide.at[groups + 1], local.at[groups + 1]))
    own = pltpu.make_async_copy(lat, full.at[f], local.at[slots])
    ctx_in = [
        pltpu.make_async_copy(ctx.at[pl.ds(n * rows, rows)], full.at[tp + n], local.at[slots + 1 + n]) for n in range(2)
    ]
    greet(others("tp", tp) + others("sp", sp))
    gather = Gather(tp, lat, full, send, recv)
    gather.start()
    for item in ctx_in + [own] + copies[::-1]:
        item.start()
    mod_in.wait()
    first_sum = jnp.dot(cond[...], mod_wide[...], preferred_element_type=F32)
    partial[...] = first_sum
    parts[s] = first_sum
    sends = []
    for step in range(1, sp):
        sends.append(remote(partial, parts.at[s], psend, precv, step - 1, "sp", lax.rem(s + step, sp)))
    for item in sends:
        item.start()
    for n in range(slots):
        row = (q_gain if n < groups else k_gain)[...]
        gains[n] = jnp.concatenate([row] * (width // head), axis=1) if width > head else row
    for step in range(1, sp):
        origin = lax.rem(s - step + sp, sp)
        remote(parts.at[origin], parts.at[origin], psend, precv, step - 1, "sp", origin).wait_recv()
    summed = parts[0]
    for n in range(1, sp):
        summed = summed + parts[n]
    total[...] = summed
    here = pl.ds(pl.multiple_of(f * mcols, mcols), mcols)
    mod[:, here] = summed
    outs = []
    for step in range(1, tp):
        outs.append(remote(total, mod.at[:, here], msend, mrecv, step - 1, "tp", lax.rem(f + step, tp)))
    for item in outs:
        item.start()
    gather.second()
    top[...] = jnp.full(top.shape, -1e30, F32)
    acc[...] = jnp.zeros(acc.shape, F32)
    for step in range(1, tp):
        origin = lax.rem(f - step + tp, tp)
        ref = mod.at[:, pl.ds(pl.multiple_of(origin * mcols, mcols), mcols)]
        remote(ref, ref, msend, mrecv, step - 1, "tp", origin).wait_recv()
    for r in range(2):
        gsc[r] = gain[...] * (1.0 + mod[r : r + 1, model : 2 * model])
        shf[r] = mod[r : r + 1, :model]
    gate[...] = mod[0:1, 2 * model :]
    gather.relay()
    for item in ctx_in + copies:
        item.wait()
    own.wait()

    ring = sp == 4
    right, left, far = (s + 1) % sp, (s + sp - 1) % sp, (s + 2) % sp

    def tile_first(number):
        if isinstance(number, int):
            return lat_rows if number == 0 else pl.multiple_of(gather.chip(number - 1) * tile, tile)
        chip = jnp.where(number == 0, tp // 2, gather.chip(jnp.maximum(number - 1, 0)))
        return pl.multiple_of(chip * tile, tile)

    def ring_copy(number, index):
        which, origin, peer = {
            0: (0, s, right), 1: (1, s, right), 2: (1, s, left), 3: (0, s, left), 4: (0, left, right), 5: (1, right, left),
        }[index]
        ref = kvs.at[origin, which, pl.ds(tile_first(number), tile)]
        return remote(ref, ref, zsend, zrecv, number * 6 + index, "sp", peer)

    def ring_wait(number, index):
        which, origin = {0: (0, left), 1: (1, left), 2: (1, right), 3: (0, right), 4: (0, far), 5: (1, far)}[index]
        ref = kvs.at[origin, which, pl.ds(tile_first(number), tile)]
        remote(ref, ref, zsend, zrecv, number * 6 + index, "sp", right).wait_recv()

    def forward(number):
        ring_wait(number, 0)
        ring_copy(number, 4).start()
        ring_wait(number, 2)
        ring_copy(number, 5).start()

    def direct(step):
        return remote(kvs.at[s], kvs.at[s], zsend, zrecv, step - 1, "sp", lax.rem(s + step, sp))

    even = lax.broadcasted_iota(jnp.int32, (tile, width), 1) % 2 == 0
    same = (
        lax.broadcasted_iota(jnp.int32, (width, width), 0) // head
        == lax.broadcasted_iota(jnp.int32, (width, width), 1) // head
    )
    ones = jnp.where(same, 1.0, 0.0).astype(BF16)
    by_row = (lax.broadcasted_iota(jnp.int32, (1, 2 * head), 1) % head) // 2 < head // 4
    grid_rows = cos.shape[0] - GRID_W
    part = min(tile, GRID_W)
    step_rows = 16

    def roll(v, by):
        if width % 128 == 0:
            return pltpu.roll(v, by % width, axis=1)
        return jnp.concatenate([v[:, width - by % width :], v[:, : width - by % width]], axis=1)

    def table(ref, first, is_ctx, fill):
        pieces = []
        for k in range(tile // part):
            at = jnp.where(is_ctx == 1, 0, first + k * part)
            row = ref[pl.ds(at // GRID_W, 1), :]
            col = ref[pl.ds(pl.multiple_of(grid_rows + at % GRID_W, 8), part), :]
            pieces.append(jnp.where(by_row, row, col))
        v = jnp.concatenate(pieces, axis=0) if len(pieces) > 1 else pieces[0]
        v = jnp.where(is_ctx == 1, fill, v)
        if width > v.shape[1]:
            return jnp.concatenate([v] * (width // v.shape[1]), axis=1)
        return v[:, :width]

    def one_tile(number, unused):
        @pl.when(number > 0)
        def _():
            gather.before(number - 1)

        is_ctx = jnp.where(number == 0, 1, 0)
        first = tile_first(number)
        base = first // rows

        def norm_rows(j, unused):
            slot = base + (j * step_rows) // rows
            row = pl.multiple_of((j * step_rows) % rows, step_rows)
            v = full[slot, pl.ds(row, step_rows), :].astype(F32)
            inv = lax.rsqrt(jnp.mean(v * v, axis=-1, keepdims=True) + EPS)
            out = v * inv * gsc[is_ctx] + shf[is_ctx]
            normed[pl.ds(pl.multiple_of(j * step_rows, step_rows), step_rows), :] = out.astype(BF16)
            return unused

        lax.fori_loop(0, tile // step_rows, norm_rows, 0)

        def turned(y, n):
            sq = y * y
            hi = sq.astype(BF16)
            lo = (sq - hi.astype(F32)).astype(BF16)
            mean = jnp.dot(hi, ones, preferred_element_type=F32) + jnp.dot(lo, ones, preferred_element_type=F32)
            u = y * lax.rsqrt(mean * (1.0 / head) + EPS) * gains[n]
            other = jnp.where(even, roll(u, -1), roll(u, 1))
            return (u * table(cos, first, is_ctx, 1.0) + other * table(sin, first, is_ctx, 0.0)).astype(BF16)

        def one_slot(m, unused):
            n = (m + groups) % slots
            y = jnp.dot(normed[...], wide[n], preferred_element_type=F32)

            @pl.when(m == 1)
            def _():
                kvs[s, 1, pl.ds(first, tile), :] = y.astype(BF16)
                if ring:
                    for index in (0, 2, 1, 3):
                        ring_copy(number, index).start()

            @pl.when(m == 0)
            def _():
                kvs[s, 0, pl.ds(first, tile), :] = turned(y, n)

            @pl.when(m > 1)
            def _():
                q_all[n, pl.ds(first, tile), :] = turned(y, n)

            return unused

        lax.fori_loop(0, jnp.where(number == 0, 2, slots), one_slot, 0)
        return unused

    lax.fori_loop(0, tiles, one_tile, 0)

    if not ring:
        for step in range(1, sp):
            direct(step).start()
    group = heads // kv_heads
    q_tile = min(256, lat_rows)
    q_tiles = lat_rows // q_tile
    scale = head ** -0.5

    def block(b, unused):
        if ring:
            @pl.when(b == 0)
            def _():
                for number in range(tiles - 2):
                    forward(number)

            @pl.when(b == 1)
            def _():
                forward(tiles - 1)
                for number in range(tiles):
                    ring_wait(number, 1)

            @pl.when(b == 2)
            def _():
                for number in range(tiles):
                    ring_wait(number, 3)

            @pl.when(b == 3)
            def _():
                for number in range(tiles):
                    ring_wait(number, 4)
                    ring_wait(number, 5)

            origin = (s + jnp.where(b == 1, sp - 1, jnp.where(b == 2, 1, jnp.where(b == 3, 2, 0)))) % sp
        else:
            @pl.when(b == 1)
            def _():
                for step in range(1, sp):
                    source = lax.rem(s - step + sp, sp)
                    remote(kvs.at[source], kvs.at[source], zsend, zrecv, step - 1, "sp", source).wait_recv()

            origin = (s + b) % sp

        def q_rows(t, unused):
            if ring:
                @pl.when((b == 0) & (t == q_tiles - 1))
                def _():
                    forward(tiles - 2)

            at = pl.ds(pl.multiple_of(t * q_tile, q_tile), q_tile)
            for h in range(kv_heads):
                k = kvs[origin, 0, :, h * head : (h + 1) * head]
                v = kvs[origin, 1, :, h * head : (h + 1) * head]
                v_wide = jnp.concatenate([v, jnp.ones((keys, head), BF16)], axis=1)
                for g in range(group):
                    n = h * group + g
                    slot, lane = (n * head) // width, (n * head) % width
                    q = q_all[slot, at, lane : lane + head]
                    scores = lax.dot_general(q, k, (((1,), (1,)), ((), ())), preferred_element_type=F32)
                    scores = scores * scale
                    offset = jnp.where(lax.broadcasted_iota(jnp.int32, (1, keys), 1) >= lat_rows, lift[n], 0.0)
                    scores = scores + offset
                    before = top[n, at, :]
                    now = jnp.maximum(before, jnp.max(scores, axis=-1, keepdims=True))
                    expo = jnp.exp(scores - now)
                    keep = jnp.exp(before - now)
                    top[n, at, :] = now
                    acc[n, at, :] = acc[n, at, :] * keep + jnp.dot(expo.astype(BF16), v_wide, preferred_element_type=F32)
            return unused

        lax.fori_loop(0, q_tiles, q_rows, 0)
        return unused

    lax.fori_loop(0, sp, block, 0)

    def close(t, unused):
        at = pl.ds(pl.multiple_of(t * q_tile, q_tile), q_tile)
        for pair in range(heads // 2):
            two = [acc[2 * pair + n, at, :] for n in range(2)]
            two = [v[:, :head] / v[:, head:] for v in two]
            attended[at, pair * 2 * head : (pair + 1) * 2 * head] = jnp.concatenate(two, axis=1).astype(BF16)
        return unused

    lax.fori_loop(0, q_tiles, close, 0)
    if ring:
        for number in range(tiles):
            for index in range(6):
                ring_copy(number, index).wait_send()
    else:
        for step in range(1, sp):
            direct(step).wait_send()
    for item in sends + outs:
        item.wait_send()
    gather.finish()


def back_kernel(tp, att, weight, out, full, wide, total, mixed, landed, send, recv, asend, arecv, local):
    f = lax.axis_index("tp")
    rows, cols = att.shape
    own_rows = out.shape[0]
    out_cols = weight.shape[1]
    load = pltpu.make_async_copy(weight, wide, local.at[0])
    load.start()
    mine = pltpu.make_async_copy(att, full.at[f], local.at[1])
    mine.start()
    greet(others("tp", tp))
    gather = Gather(tp, att, full, send, recv)
    gather.start()
    gather.second()
    total[...] = jnp.zeros(total.shape, F32)
    gather.relay()
    mine.wait()
    load.wait()
    r_tile = min(256, rows)

    def chip_step(index, unused):
        gather.before(index)
        chip = gather.chip(index)

        def row_step(t, unused):
            at = pl.ds(pl.multiple_of(t * r_tile, r_tile), r_tile)
            value = total[at, :]
            for n in range(2):
                source = chip * 2 + n
                depth = pl.ds(pl.multiple_of(source * cols, cols), cols)
                value = value + jnp.dot(full[source, at, :], wide[depth, :], preferred_element_type=F32)
            total[at, :] = value
            return unused

        lax.fori_loop(0, rows // r_tile, row_step, 0)
        return unused

    lax.fori_loop(0, tp // 2, chip_step, 0)
    for peer in range(tp):
        mixed[peer] = total[peer * own_rows : (peer + 1) * own_rows, :].astype(BF16)
    sends = []
    for step in range(1, tp):
        peer = lax.rem(f + step, tp)
        sends.append(remote(mixed.at[peer], landed.at[f], asend, arecv, step - 1, "tp", peer))
    for item in sends:
        item.start()
    landed[f] = mixed[f]
    for step in range(1, tp):
        origin = lax.rem(f - step + tp, tp)
        remote(landed.at[origin], landed.at[origin], asend, arecv, step - 1, "tp", origin).wait_recv()
    for n in range(tp):
        out[:, n * out_cols : (n + 1) * out_cols] = landed[n]
    for item in sends:
        item.wait_send()
    gather.finish()


def tables(first, count, head):
    freqs = head // 4
    lane = jnp.arange(2 * head, dtype=jnp.int32) % head
    inverse = 10000.0 ** (-(lane // 2 % freqs).astype(F32) / freqs)
    sign = jnp.where(lane % 2 == 0, -1.0, 1.0)
    grid_rows = -(-(count // GRID_W) // 8) * 8
    index = jnp.arange(grid_rows + GRID_W, dtype=jnp.int32)
    spot = jnp.where(index < grid_rows, index + first // GRID_W, index - grid_rows)
    angles = spot.astype(F32)[:, None] * inverse
    return jnp.cos(angles), jnp.sin(angles) * sign


def local(sp, tp, latent, context, condition, context_cond, mod_weight, norm_gain, query_weight, key_weight,
          value_weight, out_weight, query_gain, key_gain, context_lift):
    rows, model = latent.shape
    ctx_rows = context.shape[0]
    head = query_gain.shape[0]
    heads = query_weight.shape[1] // head
    kv_heads = key_weight.shape[1] // head
    width = key_weight.shape[1]
    slots = query_weight.shape[1] // width + 2
    block = rows * tp
    keys = block + ctx_rows
    limit = 60 * 1024 * 1024
    cond_pair = jax.nn.silu(jnp.stack([condition, context_cond])).astype(BF16)
    mcols = mod_weight.shape[1]
    cos, sin = tables(lax.axis_index("sp") * block, block, head)
    stacked = width % 128 != 0
    weights = [query_weight, key_weight, value_weight]
    if stacked:
        weights = [jnp.stack([query_weight[:, n * width : (n + 1) * width] for n in range(slots - 2)] + weights[1:])]
    dma = pltpu.SemaphoreType.DMA
    count = gather_sems(tp)
    pieces = (tp // 2 + 1) * 6 if sp == 4 else sp - 1
    attended, gate = pl.pallas_call(
        functools.partial(front_kernel, sp, tp, heads, kv_heads, head, stacked),
        name="front",
        out_shape=(jax.ShapeDtypeStruct((block, heads * head), BF16), jax.ShapeDtypeStruct((1, model), F32)),
        in_specs=[ANY, ANY, VMEM, ANY, VMEM, VMEM, VMEM, VMEM, VMEM, SMEM] + [ANY] * len(weights),
        out_specs=(VMEM, VMEM),
        scratch_shapes=[
            pltpu.VMEM((tp + 2, rows, model), BF16),
            pltpu.VMEM((2 * rows, model), BF16),
            pltpu.VMEM((slots, model, width), BF16),
            pltpu.VMEM(mod_weight.shape, BF16),
            pltpu.VMEM((sp, 2, mcols), F32),
            pltpu.VMEM((2, mcols), F32),
            pltpu.VMEM((2, mcols), F32),
            pltpu.VMEM((2, mcols * tp), F32),
            pltpu.VMEM((2, 1, model), F32),
            pltpu.VMEM((2, 1, model), F32),
            pltpu.VMEM((slots, 1, width), F32),
            pltpu.VMEM((slots - 2, block, width), BF16),
            pltpu.VMEM((sp, 2, keys, width), BF16),
            pltpu.VMEM((heads, block, 1), F32),
            pltpu.VMEM((heads, block, 2 * head), F32),
            dma((count,)), dma((count,)), dma((sp - 1,)), dma((sp - 1,)), dma((tp - 1,)), dma((tp - 1,)),
            dma((pieces,)), dma((pieces,)),
            dma((slots + 4,)),
        ],
        compiler_params=pltpu.CompilerParams(collective_id=0, has_side_effects=True, vmem_limit_bytes=limit),
    )(latent, context, cond_pair, mod_weight, norm_gain.reshape(1, model), cos, sin, query_gain.reshape(1, head),
      key_gain.reshape(1, head), context_lift, *weights)
    mixed = pl.pallas_call(
        functools.partial(back_kernel, tp),
        name="back",
        out_shape=jax.ShapeDtypeStruct((rows, model), BF16),
        in_specs=[VMEM, ANY],
        out_specs=VMEM,
        scratch_shapes=[
            pltpu.VMEM((tp, block, heads * head), BF16),
            pltpu.VMEM(out_weight.shape, BF16),
            pltpu.VMEM((block, out_weight.shape[1]), F32),
            pltpu.VMEM((tp, rows, out_weight.shape[1]), BF16),
            pltpu.VMEM((tp, rows, out_weight.shape[1]), BF16),
            dma((count,)), dma((count,)), dma((tp - 1,)), dma((tp - 1,)), dma((2,)),
        ],
        compiler_params=pltpu.CompilerParams(collective_id=2, has_side_effects=True, vmem_limit_bytes=limit),
    )(attended, out_weight)
    return (latent.astype(F32) + gate * mixed.astype(F32)).astype(BF16)


def solution(mesh):
    return jax.shard_map(
        functools.partial(local, mesh.shape["sp"], mesh.shape["tp"]),
        mesh=mesh,
        in_specs=(
            P(("sp", "tp"), None),
            P("sp", None),
            P("sp"),
            P("sp"),
            P("sp", "tp"),
            P(),
            P(None, "tp"),
            P(None, "tp"),
            P(None, "tp"),
            P(None, "tp"),
            P(),
            P(),
            P("tp"),
        ),
        out_specs=P(("sp", "tp"), None),
        check_vma=False,
    )
```

time: 143 us -> 114 us (0.80)
  Pallas kernels: 134 us -> 109 us
  local copies, waits for them, and re-layouts: 5.63 us -> 0.01 us
  other arithmetic: 0.38 us -> 4.17 us
  matrix products: 1.82 us -> 0 us
    pallas_call x2 -> x1, Pallas kernels: 101 us -> 75.4 us  [local(): pl.pallas_call(functools.partial(front_kernel, sp, tp, heads, kv_heads, h...]
    convert_element_type x1 -> x3, other arithmetic: 0.08 us -> 3.3 us  [the longest x1 1.99 us: local(): return (latent.astype(F32) + gate * mixed.astype(F32)).astype(BF16)]
    unnamed x3 -> x4, local copies, waits for them, and re-layouts: 1.87 us -> 0.01 us
    dot_general x1 -> x0, matrix products: 1.82 us -> none  [local(): partial = jnp.dot(cond_pair, mod_weight, preferred_element_type=F32)]
    another operation x4 -> x0, local copies, waits for them, and re-layouts: 1.63 us -> none  [the longest x1 0.81 us: local(): jnp.tile(query_gain, width // head)]
    concatenate x2 -> x0, local copies, waits for them, and re-layouts: 1.51 us -> none  [spread(): return jnp.concatenate([both, jnp.full((extra, 2 * head), fill, F32)])]
where the time goes in v2:
time: 114 us
  Pallas kernels  109 us (96%)
  other arithmetic  4.17 us (4%)
    pallas_call x1, Pallas kernels, local(): pl.pallas_call(functools.partial(front_kernel, sp, tp, heads, kv_heads, h...  75.4 us
    pallas_call x1, Pallas kernels, local(): pl.pallas_call(functools.partial(back_kernel, tp), name='back', out_shape...  33.9 us

profile of v2, /device:TPU:1, one launch (start us, length us, event | category | flops | bytes accessed | tf_op | source)
XLA Modules:
  0.0 113.6 jit_solution(17939007109514012258)
XLA Ops:
  0.0 1.3 %fusion.1.cond = bf16[2,1024]{1,0:T(2,128)(2,1)} fusion(f32[1,1024]{1,0:T(1,128)} %bitcast.8, f32[1,1024]{1,0:T(1,128)} %bitcast.9), kind=kLoop, calls=%fused_computation.6 | loop fusion | flops 12288 | bytes 12288 | tf_op jit(solution)/shard_map/convert_element_type | solution.py:519
  1.3 0.8 fusion
  2.2 75.4 %front.1 = (bf16[512,512]{1,0:T(8,128)(2,1)}, f32[1,4096]{1,0:T(1,128)}) custom-call(bf16[64,4096]{1,0:T(8,128)(2,1)} %lat.1, bf16[128,4096]{1,0:T(8,128)(2,1)} %ctx.1, bf16[2,1024]{1,0:T(2,128)(2,1)} %fusion.1.cond, bf16[1024,1536]{1,0:T(8,128)(2,1)} %mod_weight.1, f32[1,4096]{1,0:T(1,128)} %bitcast.6, f32[72,128]{1,0:T(8,128)} %get-tuple-element.10.cos, ...), custom_call_target="tpu_custom_call" | custom-call | tf_op jit(solution)/shard_map/front/pallas_call | solution.py:529
  77.6 0.0 copy-start
  77.6 0.0 copy-start.1
  77.7 33.9 %back.1 = bf16[64,4096]{1,0:T(8,128)(2,1)} custom-call(bf16[512,512]{1,0:T(8,128)(2,1)} %get-tuple-element.8.att, bf16[4096,512]{1,0:T(8,128)(2,1)} %weight.1), custom_call_target="tpu_custom_call" | custom-call | tf_op jit(solution)/shard_map/back/pallas_call | solution.py:558
  111.6 0.0 copy-done
  111.6 0.0 copy-done.1
  111.6 2.0 %add_convert_fusion = bf16[64,4096]{1,0:T(8,128)(2,1)} fusion(bf16[64,4096]{1,0:T(8,128)(2,1)} %back.1, bf16[64,4096]{1,0:T(8,128)(2,1)S(1)} %copy-done, f32[4096]{0:T(1024)S(1)} %bitcast.7), kind=kLoop, calls=%fused_computation | loop fusion | flops 1310720 | bytes 1589248 | tf_op jit(solution)/shard_map/convert_element_type | solution.py:574
  (2 shorter events, 0.0 us)
Async XLA Ops:
  77.6 34.0 %copy-start = (bf16[64,4096]{1,0:T(8,128)(2,1)S(1)}, bf16[64,4096]{1,0:T(8,128)(2,1)}, u32[]{:S(2)}) copy-start(bf16[64,4096]{1,0:T(8,128)(2,1)} %lat.1) | copy-start | bytes 1572868
  77.6 33.9 %copy-start.1 = (f32[1,4096]{1,0:T(1,128)S(1)}, f32[1,4096]{1,0:T(1,128)}, u32[]{:S(2)}) copy-start(f32[1,4096]{1,0:T(1,128)} %get-tuple-element.7) | copy-start | bytes 49156

commit v3 on v2

--- a/solution.py
+++ b/solution.py
@@ -166,6 +166,7 @@
     keys = kvs.shape[2]
     mcols = partial.shape[1]
     tiles = tp // 2 + 1
+    scale = head ** -0.5
     mod_in = pltpu.make_async_copy(mod_weight, mod_wide, local.at[slots + 3])
     mod_in.start()
     copies = []
@@ -195,7 +196,7 @@
     for item in sends:
         item.start()
     for n in range(slots):
-        row = (q_gain if n < groups else k_gain)[...]
+        row = q_gain[...] * scale if n < groups else k_gain[...]
         gains[n] = jnp.concatenate([row] * (width // head), axis=1) if width > head else row
     for step in range(1, sp):
         origin = lax.rem(s - step + sp, sp)
@@ -347,7 +348,6 @@
     group = heads // kv_heads
     q_tile = min(256, lat_rows)
     q_tiles = lat_rows // q_tile
-    scale = head ** -0.5
 
     def block(b, unused):
         if ring:
@@ -399,9 +399,7 @@
                     slot, lane = (n * head) // width, (n * head) % width
                     q = q_all[slot, at, lane : lane + head]
                     scores = lax.dot_general(q, k, (((1,), (1,)), ((), ())), preferred_element_type=F32)
-                    scores = scores * scale
-                    offset = jnp.where(lax.broadcasted_iota(jnp.int32, (1, keys), 1) >= lat_rows, lift[n], 0.0)
-                    scores = scores + offset
+                    scores = jnp.concatenate([scores[:, :lat_rows], scores[:, lat_rows:] + lift[n]], axis=1)
                     before = top[n, at, :]
                     now = jnp.maximum(before, jnp.max(scores, axis=-1, keepdims=True))
                     expo = jnp.exp(scores - now)

time: 114 us -> 114 us (level)
  no operation moved by 1% of the time
where the time goes in v3:
time: 114 us; the launch traced here: 113 us
  Pallas kernels  109 us (96%)
  other arithmetic  4.17 us (4%)
    pallas_call x1, Pallas kernels, local(): pl.pallas_call(functools.partial(front_kernel, sp, tp, heads, kv_heads, h...  75.1 us
    pallas_call x1, Pallas kernels, local(): pl.pallas_call(functools.partial(back_kernel, tp), name='back', out_shape...  33.9 us

profile of v3, /device:TPU:1, one launch (start us, length us, event | category | flops | bytes accessed | tf_op | source)
XLA Modules:
  0.0 113.3 jit_solution(5893904971680314532)
XLA Ops:
  0.0 1.3 %fusion.1.cond = bf16[2,1024]{1,0:T(2,128)(2,1)} fusion(f32[1,1024]{1,0:T(1,128)} %bitcast.8, f32[1,1024]{1,0:T(1,128)} %bitcast.9), kind=kLoop, calls=%fused_computation.6 | loop fusion | flops 12288 | bytes 12288 | tf_op jit(solution)/shard_map/convert_element_type | solution.py:517
  1.3 0.8 fusion
  2.2 75.1 %front.1 = (bf16[512,512]{1,0:T(8,128)(2,1)}, f32[1,4096]{1,0:T(1,128)}) custom-call(bf16[64,4096]{1,0:T(8,128)(2,1)} %lat.1, bf16[128,4096]{1,0:T(8,128)(2,1)} %ctx.1, bf16[2,1024]{1,0:T(2,128)(2,1)} %fusion.1.cond, bf16[1024,1536]{1,0:T(8,128)(2,1)} %mod_weight.1, f32[1,4096]{1,0:T(1,128)} %bitcast.6, f32[72,128]{1,0:T(8,128)} %get-tuple-element.10.cos, ...), custom_call_target="tpu_custom_call" | custom-call | tf_op jit(solution)/shard_map/front/pallas_call | solution.py:527
  77.3 0.0 copy-start
  77.3 0.0 copy-start.1
  77.3 33.9 %back.1 = bf16[64,4096]{1,0:T(8,128)(2,1)} custom-call(bf16[512,512]{1,0:T(8,128)(2,1)} %get-tuple-element.8.att, bf16[4096,512]{1,0:T(8,128)(2,1)} %weight.1), custom_call_target="tpu_custom_call" | custom-call | tf_op jit(solution)/shard_map/back/pallas_call | solution.py:556
  111.2 0.0 copy-done
  111.3 0.0 copy-done.1
  111.3 2.0 %add_convert_fusion = bf16[64,4096]{1,0:T(8,128)(2,1)} fusion(bf16[64,4096]{1,0:T(8,128)(2,1)} %back.1, bf16[64,4096]{1,0:T(8,128)(2,1)S(1)} %copy-done, f32[4096]{0:T(1024)S(1)} %bitcast.7), kind=kLoop, calls=%fused_computation | loop fusion | flops 1310720 | bytes 1589248 | tf_op jit(solution)/shard_map/convert_element_type | solution.py:572
  (2 shorter events, 0.0 us)
Async XLA Ops:
  77.3 33.9 %copy-start = (bf16[64,4096]{1,0:T(8,128)(2,1)S(1)}, bf16[64,4096]{1,0:T(8,128)(2,1)}, u32[]{:S(2)}) copy-start(bf16[64,4096]{1,0:T(8,128)(2,1)} %lat.1) | copy-start | bytes 1572868
  77.3 33.9 %copy-start.1 = (f32[1,4096]{1,0:T(1,128)S(1)}, f32[1,4096]{1,0:T(1,128)}, u32[]{:S(2)}) copy-start(f32[1,4096]{1,0:T(1,128)} %get-tuple-element.7) | copy-start | bytes 49156
